TPU v7x, 32 devices: a whole 2x2x4 slice. The times are simulated.
32 devices in a mesh: ep: 8 (over z, x), tp: 4 (over y, core).
Axes of the slice: x: 2, y: 2, z: 4, core: 2. Of those that a mesh axis runs over, the one named last changes fastest.
Arguments:
- hidden_in: bfloat16 [128, 4096], P('ep'), may hold values from -6 to 6
- w_query: bfloat16 [4096, 2048], P('ep', 'tp'), may hold values from -0.09375 to 0.09375
- w_key: bfloat16 [4096, 2048], P('ep', 'tp'), may hold values from -0.09375 to 0.09375
- w_value: bfloat16 [4096, 2048], P('ep', 'tp'), may hold values from -0.09375 to 0.09375
- w_outgate: bfloat16 [4096, 2048], P('ep', 'tp'), may hold values from -0.09375 to 0.09375
- w_igate: bfloat16 [4096, 16], P('ep', 'tp'), may hold values from -0.09375 to 0.09375
- w_fgate: bfloat16 [4096, 16], P('ep', 'tp'), may hold values from -0.09375 to 0.09375
- input_bias: float32 [16], P('tp'), may hold values from -3 to 303
- forget_bias: float32 [16], P('tp'), may hold values from -1 to 5
- mem_state: float32 [128, 16, 16384], P('ep', 'tp'), may hold values from -4 to 4
- max_state: float32 [128, 16], P('ep', 'tp'), may hold values from -4 to 304
- head_gain: float32 [2048], P('tp'), may hold values from 0.1 to 1.9
- w_output: bfloat16 [2048, 4096], P('tp'), may hold values from -0.26367188 to 0.26367188
- first_gain: float32 [4096], replicated, may hold values from 0.35 to 3.25
- w_group_router: bfloat16 [4096, 2], replicated, may hold values from -0.09375 to 0.09375
- w_expert_router: bfloat16 [4096, 8], replicated, may hold values from -0.09375 to 0.09375
- expert_route: int32 [128, 2], P('ep'), may hold values from 0 to 7, as said below
- w_expgate: bfloat16 [8, 4096, 1024], P('ep', None, 'tp'), may hold values from -0.09375 to 0.09375
- w_expup: bfloat16 [8, 4096, 1024], P('ep', None, 'tp'), may hold values from -0.09375 to 0.09375
- w_expdown: bfloat16 [8, 1024, 4096], P('ep', 'tp'), may hold values from -0.75 to 0.75
- second_gain: float32 [4096], P('tp'), may hold values from 0.1 to 1.9
Outputs:
- hidden_out: bfloat16 [128, 4096], P('ep', 'tp')
- mem_next: float32 [128, 16, 16384], P('ep', 'tp')
- max_next: float32 [128, 16], P('ep', 'tp')
Inputs may be any that keep to these rules, and one draw needn't show every extreme that they name: `expert_route`: each row names two different experts of one group (an expert's group is its number divided by 4). In each aligned block of 16 rows (the rows of one index of ep) every group is named by exactly 8 rows, no expert by more than 8 rows, and some expert by exactly 8 rows.
All inputs are finite; a program needn't handle non-finite values.
Results may differ from a plain program's by a relative error of at most 0.02.
Values may be sent and summed in bfloat16 or wider, within the bound.
A program may use at most 64 MiB of HBM per device.

v0:
```python
import jax
import jax.numpy as jnp
from jax import lax
from jax.sharding import PartitionSpec as P

D = 4096
DH = 128
GROUP_SIZE = 4
res_alpha = 8.0**0.25


def layer_norm(values, gain):
    row_mean = jnp.mean(values, -1, keepdims=True)
    row_var = jnp.mean(values * values, -1, keepdims=True) - row_mean * row_mean
    return (values - row_mean) * lax.rsqrt(row_var + 1e-05) * gain


def mlstm_step(queries, keys_scaled, values, log_input, log_forget, memory, stabilizer):
    new_max = jnp.maximum(log_forget + stabilizer, log_input)
    keep_old = jnp.exp(log_forget + stabilizer - new_max)
    write_new = jnp.exp(log_input - new_max)
    scores = jnp.sum(queries * keys_scaled, -1) * write_new
    read_old = jnp.einsum("bhd,bhde->bhe", queries, memory, precision=lax.Precision.HIGHEST)
    readout = scores[..., None] * values + keep_old[..., None] * read_old
    memory_next = (
        keep_old[..., None, None] * memory
        + write_new[..., None, None] * keys_scaled[..., :, None] * values[..., None, :]
    )
    return (readout, memory_next, new_max)


def head_mix(readout, head_gain, out_pre):
    scaled = readout * lax.rsqrt(jnp.mean(readout * readout, -1, keepdims=True) + 1e-06)
    flat_heads = scaled.reshape(scaled.shape[0], -1)
    return (flat_heads * head_gain * jax.nn.sigmoid(out_pre)).astype(jnp.bfloat16)


def route_weights(mid_float, w_group_router, w_expert_router, expert_route):
    group_logits = jnp.dot(
        mid_float, w_group_router.astype(jnp.float32), precision=lax.Precision.HIGHEST
    )
    expert_logits = jnp.dot(
        mid_float, w_expert_router.astype(jnp.float32), precision=lax.Precision.HIGHEST
    )
    first_expert = expert_route[:, 0]
    second_expert = expert_route[:, 1]
    expert_ids = lax.broadcasted_iota(jnp.int32, expert_logits.shape, 1)
    group_ids = lax.broadcasted_iota(jnp.int32, group_logits.shape, 1)
    first_logit = jnp.sum(jnp.where(expert_ids == first_expert[:, None], expert_logits, 0.0), -1)
    second_logit = jnp.sum(jnp.where(expert_ids == second_expert[:, None], expert_logits, 0.0), -1)
    group_pick = jnp.sum(
        jnp.where(group_ids == (first_expert // GROUP_SIZE)[:, None], group_logits, 0.0), -1
    )
    group_gate = jax.nn.sigmoid(group_pick)
    return (
        group_gate * jax.nn.sigmoid(first_logit - second_logit),
        group_gate * jax.nn.sigmoid(second_logit - first_logit),
    )


def slot_ranks(flat_routes, expert_total):
    onehot = (
        flat_routes[:, None]
        == lax.broadcasted_iota(jnp.int32, (flat_routes.shape[0], expert_total), 1)
    ).astype(jnp.int32)
    running = jnp.cumsum(onehot, 0)
    return jnp.sum((running - 1) * onehot, -1)


def body(
    hidden_in,
    w_query,
    w_key,
    w_value,
    w_outgate,
    w_igate,
    w_fgate,
    input_bias,
    forget_bias,
    mem_state,
    max_state,
    head_gain,
    w_output,
    first_gain,
    w_group_router,
    w_expert_router,
    expert_route,
    w_expgate,
    w_expup,
    w_expdown,
    second_gain,
):
    own_rows, width = hidden_in.shape
    heads_here = mem_state.shape[1]
    head_width = heads_here * DH
    top_count = expert_route.shape[1]
    spread_rows = lax.all_to_all(hidden_in, "ep", split_axis=1, concat_axis=0, tiled=True)
    stacked_w = jnp.concatenate([w_query, w_key, w_value, w_outgate], 1)
    gate_w = jnp.concatenate([w_igate, w_fgate], 1)
    proj_terms = jnp.dot(spread_rows, stacked_w, preferred_element_type=jnp.float32)
    gate_terms = jnp.dot(spread_rows, gate_w, preferred_element_type=jnp.float32)
    projected, gate_sums = (
        lax.psum_scatter(proj_terms, "ep", scatter_dimension=0, tiled=True),
        lax.psum_scatter(gate_terms, "ep", scatter_dimension=0, tiled=True),
    )
    shaped = projected.reshape(own_rows, 4, heads_here, DH)
    queries = shaped[:, 0]
    keys_raw = shaped[:, 1]
    values = shaped[:, 2]
    out_pre = shaped[:, 3].reshape(own_rows, head_width)
    input_sum = gate_sums[:, :heads_here]
    forget_sum = gate_sums[:, heads_here:]
    keys_scaled = keys_raw * DH ** (-0.5)
    log_input = input_sum + input_bias
    log_forget = jax.nn.log_sigmoid(forget_sum + forget_bias)
    memory = mem_state.reshape(own_rows, heads_here, DH, DH)
    readout, memory_square, new_max = mlstm_step(
        queries, keys_scaled, values, log_input, log_forget, memory, max_state
    )
    memory_next = memory_square.reshape(own_rows, heads_here, DH * DH)
    mixed_heads = head_mix(readout, head_gain, out_pre)
    partial_mix = jnp.dot(mixed_heads, w_output, preferred_element_type=jnp.float32).astype(
        jnp.bfloat16
    )
    mix = lax.psum(partial_mix.astype(jnp.float32).astype(jnp.bfloat16), "tp").astype(jnp.float32)
    mid_float = layer_norm(res_alpha * hidden_in.astype(jnp.float32) + mix, first_gain)
    mid = mid_float.astype(jnp.bfloat16)
    first_weight, second_weight = route_weights(
        mid_float, w_group_router, w_expert_router, expert_route
    )
    expert_total = w_expgate.shape[0] * lax.axis_size("ep")
    capacity = 2 * own_rows * top_count // expert_total
    flat_routes = expert_route.reshape(-1)
    local_slot = flat_routes * capacity + slot_ranks(flat_routes, expert_total)
    share_width = width // lax.axis_size("tp")
    mid_share = lax.dynamic_slice_in_dim(mid, lax.axis_index("tp") * share_width, share_width, 1)
    buffer = (
        jnp.zeros((expert_total * capacity, width), jnp.bfloat16)
        .at[local_slot]
        .set(jnp.repeat(mid, top_count, 0))
    )
    arrived = lax.all_to_all(
        buffer.reshape(expert_total, capacity, width), "ep", split_axis=0, concat_axis=1, tiled=True
    )
    gate_pre = jnp.einsum("erd,edf->erf", arrived, w_expgate, preferred_element_type=jnp.float32)
    up_pre = jnp.einsum("erd,edf->erf", arrived, w_expup, preferred_element_type=jnp.float32)
    hidden_units = (jax.nn.silu(gate_pre) * up_pre).astype(jnp.bfloat16)
    down_terms = jnp.einsum(
        "erf,efd->erd", hidden_units, w_expdown, preferred_element_type=jnp.float32
    ).astype(jnp.bfloat16)
    expert_share = lax.psum_scatter(
        down_terms.astype(jnp.float32).astype(jnp.bfloat16), "tp", scatter_dimension=2, tiled=True
    )
    returned = lax.all_to_all(expert_share, "ep", split_axis=1, concat_axis=0, tiled=True)
    picked = returned.reshape(expert_total * capacity, share_width)[local_slot]
    picked = picked.astype(jnp.float32).reshape(own_rows, top_count, share_width)
    moe = first_weight[:, None] * picked[:, 0] + second_weight[:, None] * picked[:, 1]
    joined = res_alpha * mid_share.astype(jnp.float32) + moe
    row_sum, square_sum = lax.psum((jnp.sum(joined, -1), jnp.sum(joined * joined, -1)), "tp")
    row_mean = row_sum / D
    row_var = square_sum / D - row_mean * row_mean
    hidden_out = (
        (joined - row_mean[:, None]) * lax.rsqrt(row_var[:, None] + 1e-05) * second_gain
    ).astype(jnp.bfloat16)
    return (hidden_out, memory_next, new_max)


def solution(mesh):
    return jax.shard_map(
        body,
        mesh=mesh,
        in_specs=(
            P("ep", None),
            P("ep", "tp"),
            P("ep", "tp"),
            P("ep", "tp"),
            P("ep", "tp"),
            P("ep", "tp"),
            P("ep", "tp"),
            P("tp"),
            P("tp"),
            P("ep", "tp", None),
            P("ep", "tp"),
            P("tp"),
            P("tp", None),
            P(),
            P(),
            P(),
            P("ep", None),
            P("ep", None, "tp"),
            P("ep", None, "tp"),
            P("ep", "tp", None),
            P("tp"),
        ),
        out_specs=(P("ep", "tp"), P("ep", "tp", None), P("ep", "tp")),
        check_vma=False,
    )
```

profile of v0, /device:TPU:0, one launch (start us, length us, event | category | flops | bytes accessed | tf_op | source)
XLA Modules:
  0.0 277.9 jit_solution(14590576950777728029)
XLA Ops:
  7.2 1.1 copy.139
  8.3 14.4 %all_to_all.37 = bf16[16,8,512]{2,0,1:T(8,128)(2,1)S(1)} all-to-all(bf16[16,8,512]{2,0,1:T(8,128)(2,1)S(1)} %bitcast.124), channel_id=1, replica_groups=mesh['ep'=8,'tp'=4] {'ep'}, dimensions={1} | all-to-all | bytes 262144 | tf_op jit(solution)/shard_map/all_to_all | solution.py:97
  22.7 0.8 convolution_bitcast_fusion.1
  23.5 0.7 copy.106
  24.4 2.3 convolution_bitcast_fusion
  26.6 1.3 copy.104
  28.1 6.1 %reshape.183 = f32[16,4,128,128]{3,2,1,0:T(8,128)} reshape(f32[16,4,16384]{2,1,0:T(4,128)} %param.30) | data formatting | bytes 8388608 | tf_op jit(solution)/shard_map/reshape | solution.py:116
  34.7 0.2 select_reduce_fusion
  34.9 49.9 %reduce-scatter.12.cloned.1.call-done = f32[16,8]{1,0:T(8,128)} async-done(((f32[128,8]{1,0:T(8,128)}), f32[16,8]{1,0:T(8,128)}) %reduce-scatter.12.cloned.1.call-update) | async-done | bytes 528 | tf_op jit(solution)/shard_map/reduce_scatter | solution.py:104
  84.8 0.9 broadcast_multiply_fusion.2
  85.7 66.2 %reduce-scatter.10.cloned.1.call-done = f32[16,2048]{1,0:T(8,128)} async-done(((f32[128,2048]{1,0:T(8,128)}), f32[16,2048]{1,0:T(8,128)}) %reduce-scatter.10.cloned.1.call-update) | async-done | bytes 131088
  151.8 1.2 copy.105
  153.1 0.9 fusion.62
  154.0 1.0 copy.109
  155.1 1.1 copy.110
  156.1 1.1 copy.111
  157.2 0.1 bitcast_multiply_fusion.2
  157.3 5.3 %fusion.64 = f32[16,4,1,128]{3,2,1,0:T(1,128)S(1)} fusion(f32[16,4,128,1]{2,3,1,0:T(1,128)S(1)} %bitcast.125, f32[16,4,128,128]{3,2,1,0:T(8,128)} %reshape.183), kind=kOutput, calls=%fused_computation.111 | convolution fusion | flops 12582912 | bytes 4259840 | tf_op jit(solution)/shard_map/bhd,bhde->bhe/dot_general | solution.py:23
  162.8 0.2 multiply_reduce_fusion.2
  163.0 0.1 broadcast_multiply_fusion.1
  163.3 3.5 %convolution_convert_fusion.1 = bf16[16,4096]{1,0:T(8,128)(2,1)} fusion(bf16[512,4096]{1,0:T(8,128)(2,1)} %param.33, f32[2,8,4,128]{3,2,1,0:T(4,128)S(1)} %bitcast.128, f32[2,8,4,128]{3,2,1,0:T(4,128)S(1)} %bitcast.129, f32[512]{0:T(512)S(1)} %copy-done.7), kind=kOutput, calls=%fused_computation.4 | convolution fusion | flops 67198976 | bytes 4392960 | tf_op jit(solution)/shard_map/dot_general | solution.py:122
  166.8 30.9 %all-reduce.3.cloned.1.call-done = bf16[16,4096]{1,0:T(8,128)(2,1)} async-done(((bf16[16,4096]{1,0:T(8,128)(2,1)}), bf16[16,4096]{1,0:T(8,128)(2,1)}) %all-reduce.3.cloned.1.call-update) | async-done | bytes 131088 | tf_op jit(solution)/shard_map/psum | solution.py:125
  197.7 1.1 fusion.27
  198.8 1.0 fusion.58
  199.8 0.2 broadcast_in_dim.15
  200.1 1.8 scatter_custom_fusion
  201.9 5.5 %all-to-all-start.1 = ((bf16[8,8,4096]{2,1,0:T(8,128)(2,1)}), bf16[8,8,4096]{2,1,0:T(8,128)(2,1)S(1)}, u32[]{:S(2)}, u32[]{:S(2)}) async-start(bf16[8,8,4096]{2,1,0:T(8,128)(2,1)} %bitcast.18), calls=%async_computation.1 | async-start | bytes 1048576 | tf_op jit(solution)/shard_map/all_to_all | solution.py:142
  207.5 0.7 copy.98
  208.1 2.6 broadcast_multiply_fusion
  210.8 5.6 %mul.268 = f32[16,4,16384]{2,1,0:T(4,128)} reshape(f32[16,4,128,128]{3,2,1,0:T(8,128)} %broadcast_multiply_fusion) | data formatting | bytes 8388608 | tf_op jit(solution)/shard_map/mul | solution.py:27
  216.3 4.5 %all-to-all-done.1 = bf16[8,8,4096]{2,1,0:T(8,128)(2,1)S(1)} async-done(((bf16[8,8,4096]{2,1,0:T(8,128)(2,1)}), bf16[8,8,4096]{2,1,0:T(8,128)(2,1)S(1)}, u32[]{:S(2)}, u32[]{:S(2)}) %all-to-all-start.1) | async-done | bytes 524320 | tf_op jit(solution)/shard_map/all_to_all | solution.py:142
  220.8 2.0 fusion.11
  222.9 3.8 %fusion = bf16[1,64,4096]{2,1,0:T(8,128)(2,1)} fusion(bf16[1,256,4096]{2,1,0:T(8,128)(2,1)S(1)} %copy-done, bf16[1,4096,256]{2,1,0:T(8,128)(2,1)} %param.39, bf16[8,8,4096]{2,1,0:T(8,128)(2,1)S(1)} %all-to-all-done.1, f32[64,256]{1,0:T(8,128)S(1)} %fusion.11), kind=kOutput, calls=%fused_computation.3 | convolution fusion | flops 268795904 | bytes 5308416 | tf_op jit(solution)/shard_map/erf,efd->erd/dot_general | solution.py:148
  226.7 6.9 %multiply_add_fusion = f32[16,4,16384]{2,1,0:T(4,128)} fusion(f32[16,4,16384]{2,1,0:T(4,128)} %mul.268, f32[16,4,16384]{2,1,0:T(4,128)} %param.30, f32[16,4]{1,0:T(8,128)S(1)} %get-tuple-element.28), kind=kLoop, calls=%fused_computation.5 | loop fusion | flops 2097152 | bytes 12583168 | tf_op jit(solution)/shard_map/add | solution.py:26
  233.6 0.4 fusion.19
  234.0 0.4 select_reduce_fusion.2
  234.4 12.5 %reduce-scatter.8.cloned.1.call-done = bf16[1,64,1024]{2,1,0:T(8,128)(2,1)} async-done(((bf16[1,64,4096]{2,1,0:T(8,128)(2,1)}), bf16[1,64,1024]{2,1,0:T(8,128)(2,1)}) %reduce-scatter.8.cloned.1.call-update) | async-done | bytes 131088 | tf_op jit(solution)/shard_map/reduce_scatter | solution.py:151
  246.9 1.1 copy.141
  248.0 0.5 broadcast.198
  248.5 1.4 reduce
  249.9 0.7 reshape.217
  250.6 5.5 %all-to-all-start.2 = ((bf16[8,2,4096]{2,1,0:T(2,128)(2,1)}), bf16[8,2,4096]{2,1,0:T(2,128)(2,1)S(1)}, u32[]{:S(2)}, u32[]{:S(2)}) async-start(bf16[8,2,4096]{2,1,0:T(2,128)(2,1)} %reshape.217), calls=%async_computation.3 | async-start | bytes 262144 | tf_op jit(solution)/shard_map/all_to_all | solution.py:154
  256.2 7.3 %all-to-all-done.2 = bf16[8,2,4096]{2,1,0:T(2,128)(2,1)S(1)} async-done(((bf16[8,2,4096]{2,1,0:T(2,128)(2,1)}), bf16[8,2,4096]{2,1,0:T(2,128)(2,1)S(1)}, u32[]{:S(2)}, u32[]{:S(2)}) %all-to-all-start.2) | async-done | bytes 131104 | tf_op jit(solution)/shard_map/all_to_all | solution.py:154
  263.5 0.1 reshape.218
  263.7 0.6 gather_fusion
  264.5 0.2 fusion.59
  264.7 5.9 %all-reduce = (f32[16]{0:T(128)S(1)}, f32[16]{0:T(128)S(1)}) all-reduce(f32[16]{0:T(128)S(1)} %get-tuple-element.9, f32[16]{0:T(128)S(1)} %get-tuple-element.8), channel_id=1, replica_groups=mesh['ep'=8,'tp'=4] {'tp'}, use_global_device_ids=true, to_apply=%region_17.18 | all-reduce | flops 32 | bytes 256 | tf_op jit(solution)/shard_map/psum | solution.py:159
  270.7 0.7 multiply_convert_fusion
  (58 shorter events, 1.5 us)
Async XLA Ops:
  7.2 215.7 %copy-start = (bf16[1,256,4096]{2,1,0:T(8,128)(2,1)S(1)}, bf16[1,256,4096]{2,1,0:T(8,128)(2,1)}, u32[]{:S(2)}) copy-start(bf16[1,256,4096]{2,1,0:T(8,128)(2,1)} %param.40) | copy-start | bytes 6291460
  7.2 77.6 %reduce-scatter.12.cloned.1.call-start = ((), (), s32[]{:S(2)}) async-start(), calls=%async_computation.9 | async-start | bytes 73728 | tf_op jit(solution)/shard_map/reduce_scatter | solution.py:104
  24.3 3.7 %copy-start.10 = (f32[16,4]{0,1:T(4,128)S(1)}, f32[16,4]{0,1:T(4,128)}, u32[]{:S(2)}) copy-start(f32[16,4]{0,1:T(4,128)} %param.31) | copy-start | bytes 772
  24.3 127.5 %reduce-scatter.10.cloned.1.call-start = ((), (), s32[]{:S(2)}) async-start(), calls=%async_computation.8 | async-start | bytes 1179648
  28.0 169.7 %all-reduce.3.cloned.1.call-start = ((), (), s32[]{:S(2)}) async-start(), calls=%async_computation.6 | async-start | bytes 262144 | tf_op jit(solution)/shard_map/psum | solution.py:125
  28.1 6.1 %copy-start.5 = (s32[16,2]{0,1:T(2,128)S(1)}, s32[16,2]{0,1:T(2,128)}, u32[]{:S(2)}) copy-start(s32[16,2]{0,1:T(2,128)} %param.37) | copy-start | bytes 388
  28.1 56.7 %copy-start.8 = (f32[4]{0:T(128)S(1)}, f32[4]{0:T(128)}, u32[]{:S(2)}) copy-start(f32[4]{0:T(128)} %param.28) | copy-start | bytes 52
  28.1 56.7 %copy-start.9 = (f32[4]{0:T(128)S(1)}, f32[4]{0:T(128)}, u32[]{:S(2)}) copy-start(f32[4]{0:T(128)} %param.29) | copy-start | bytes 52
  85.7 77.0 %copy-start.3 = (f32[16,8]{1,0:T(8,128)S(1)}, f32[16,8]{1,0:T(8,128)}, u32[]{:S(2)}) copy-start(f32[16,8]{1,0:T(8,128)} %reduce-scatter.12.cloned.1.call-done) | copy-start | bytes 1540
  153.1 10.2 %copy-start.7 = (f32[512]{0:T(512)S(1)}, f32[512]{0:T(512)}, u32[]{:S(2)}) copy-start(f32[512]{0:T(512)} %param.32) | copy-start | bytes 6148
  157.3 40.4 %copy-start.1 = (bf16[16,4096]{1,0:T(8,128)(2,1)S(1)}, bf16[16,4096]{1,0:T(8,128)(2,1)}, u32[]{:S(2)}) copy-start(bf16[16,4096]{1,0:T(8,128)(2,1)} %param.21) | copy-start | bytes 393220
  157.3 41.5 %copy-start.4 = (f32[4096]{0:T(1024)S(1)}, f32[4096]{0:T(1024)}, u32[]{:S(2)}) copy-start(f32[4096]{0:T(1024)} %param.34) | copy-start | bytes 49156
  201.9 18.9 %all-to-all-start.1 = ((bf16[8,8,4096]{2,1,0:T(8,128)(2,1)}), bf16[8,8,4096]{2,1,0:T(8,128)(2,1)S(1)}, u32[]{:S(2)}, u32[]{:S(2)}) async-start(bf16[8,8,4096]{2,1,0:T(8,128)(2,1)} %bitcast.18), calls=%async_computation.1 | async-start | bytes 1048576 | tf_op jit(solution)/shard_map/all_to_all | solution.py:142
  207.4 39.5 %reduce-scatter.8.cloned.1.call-start = ((), (), s32[]{:S(2)}) async-start(), calls=%async_computation.7 | async-start | bytes 655360 | tf_op jit(solution)/shard_map/reduce_scatter | solution.py:151
  226.7 6.9 %copy-start.2 = (bf16[16,4096]{1,0:T(8,128)(2,1)S(1)}, bf16[16,4096]{1,0:T(8,128)(2,1)}, u32[]{:S(2)}) copy-start(bf16[16,4096]{1,0:T(8,128)(2,1)} %all-reduce.3.cloned.1.call-done) | copy-start | bytes 393220
  226.7 6.9 %copy-start.12 = (bf16[4096,2]{0,1:T(2,128)(2,1)S(1)}, bf16[4096,2]{0,1:T(2,128)(2,1)}, u32[]{:S(2)}) copy-start(bf16[4096,2]{0,1:T(2,128)(2,1)} %param.35) | copy-start | bytes 49156
  226.7 7.3 %copy-start.11 = (bf16[4096,8]{0,1:T(8,128)(2,1)S(1)}, bf16[4096,8]{0,1:T(8,128)(2,1)}, u32[]{:S(2)}) copy-start(bf16[4096,8]{0,1:T(8,128)(2,1)} %param.36) | copy-start | bytes 196612
  233.6 37.1 %copy-start.6 = (f32[1024]{0:T(1024)S(1)}, f32[1024]{0:T(1024)}, u32[]{:S(2)}) copy-start(f32[1024]{0:T(1024)} %param.41) | copy-start | bytes 12292
  250.6 12.9 %all-to-all-start.2 = ((bf16[8,2,4096]{2,1,0:T(2,128)(2,1)}), bf16[8,2,4096]{2,1,0:T(2,128)(2,1)S(1)}, u32[]{:S(2)}, u32[]{:S(2)}) async-start(bf16[8,2,4096]{2,1,0:T(2,128)(2,1)} %reshape.217), calls=%async_computation.3 | async-start | bytes 262144 | tf_op jit(solution)/shard_map/all_to_all | solution.py:154
Sparse Core Ops, SparseCore 0:
  24.4 60.3 reduce-scatter.11
  88.2 63.5 reduce-scatter.9
  166.9 30.7 all-reduce.2
  226.8 20.0 reduce-scatter.7
where the time goes:
time: 279 us; the launch traced here: 278 us
  waiting for transfers between devices  171 us (61%)
  local copies, waits for them, and re-layouts  26.8 us (10%)
  blocking collectives  20.3 us (7%)
  matrix products  18.5 us (7%)
  other arithmetic  15.7 us (6%)
  between operations  14.1 us (5%)
  starting transfers between devices  11.2 us (4%)
    unnamed x5, waiting for transfers between devices  66.2 us
    reduce_scatter x1, waiting for transfers between devices, body(): lax.psum_scatter(gate_terms, 'ep', scatter_dimension=0, tiled=True)  49.9 us
    psum x1, waiting for transfers between devices, body(): lax.psum(partial_mix.astype(jnp.float32).astype(jnp.bfloat16), 'tp')  30.9 us
    all_to_all x1, blocking collectives, body(): lax.all_to_all(hidden_in, 'ep', split_axis=1, concat_axis=0, tiled=True)  14.4 us
    reduce_scatter x1, waiting for transfers between devices, body(): lax.psum_scatter(down_terms.astype(jnp.float32).astype(jnp.bfloat16), 'tp...  12.5 us
    unnamed x40, local copies, waits for them, and re-layouts  8.86 us
    all_to_all x1, waiting for transfers between devices, body(): lax.all_to_all(expert_share, 'ep', split_axis=1, concat_axis=0, tiled=True)  7.32 us
    add x1, other arithmetic, mlstm_step(): keep_old[..., None, None] * memory  6.88 us
  transfers between devices with their start and end apart: 6, of which 6 were waited for; matrix products, arithmetic and copies ran while one was open for 10% of the time, Pallas kernels for 0%

commit v1 on v0

--- a/solution.py
+++ b/solution.py
@@ -122,7 +122,11 @@
     partial_mix = jnp.dot(mixed_heads, w_output, preferred_element_type=jnp.float32).astype(
         jnp.bfloat16
     )
-    mix = lax.psum(partial_mix.astype(jnp.float32).astype(jnp.bfloat16), "tp").astype(jnp.float32)
+    mix = (
+        lax.all_gather(partial_mix.astype(jnp.float32).astype(jnp.bfloat16), "tp")
+        .sum(axis=0)
+        .astype(jnp.float32)
+    )
     mid_float = layer_norm(res_alpha * hidden_in.astype(jnp.float32) + mix, first_gain)
     mid = mid_float.astype(jnp.bfloat16)
     first_weight, second_weight = route_weights(

time: 279 us -> 252 us (0.903)
  waiting for transfers between devices: 171 us -> 142 us
  blocking collectives: 20.3 us -> 27.5 us
    psum x1 -> x0, waiting for transfers between devices: 30.9 us -> none  [body(): lax.psum(partial_mix.astype(jnp.float32).astype(jnp.bfloat16), 'tp')]
    all_gather x0 -> x1, blocking collectives: none -> 7.14 us  [body(): lax.all_gather(partial_mix.astype(jnp.float32).astype(jnp.bfloat16), 'tp')]
    unnamed x5 -> x4, waiting for transfers between devices: 66.2 us -> 66.2 us
    unnamed x40 -> x38, local copies, waits for them, and re-layouts: 8.86 us -> 8.85 us
  transfers between devices with their start and end apart: 6 -> 5, of which waited for: 6 -> 5; matrix products, arithmetic and copies ran while one was open for 10% -> 11% of each run, Pallas kernels for 0% -> 0%
where the time goes in v1:
time: 252 us; the launch traced here: 251 us
  waiting for transfers between devices  142 us (56%)
  blocking collectives  27.5 us (11%)
  local copies, waits for them, and re-layouts  26.8 us (11%)
  matrix products  17.8 us (7%)
  between operations  14.1 us (6%)
  other arithmetic  13.9 us (6%)
  starting transfers between devices  9.37 us (4%)
    unnamed x4, waiting for transfers between devices  66.2 us
    reduce_scatter x1, waiting for transfers between devices, body(): lax.psum_scatter(gate_terms, 'ep', scatter_dimension=0, tiled=True)  49.9 us
    all_to_all x1, blocking collectives, body(): lax.all_to_all(hidden_in, 'ep', split_axis=1, concat_axis=0, tiled=True)  14.4 us
    reduce_scatter x1, waiting for transfers between devices, body(): lax.psum_scatter(down_terms.astype(jnp.float32).astype(jnp.bfloat16), 'tp...  12.5 us
    unnamed x38, local copies, waits for them, and re-layouts  8.85 us
    all_to_all x1, waiting for transfers between devices, body(): lax.all_to_all(expert_share, 'ep', split_axis=1, concat_axis=0, tiled=True)  7.32 us
    all_gather x1, blocking collectives, body(): lax.all_gather(partial_mix.astype(jnp.float32).astype(jnp.bfloat16), 'tp')  7.14 us
    add x1, other arithmetic, mlstm_step(): keep_old[..., None, None] * memory  6.86 us
  transfers between devices with their start and end apart: 5, of which 5 were waited for; matrix products, arithmetic and copies ran while one was open for 11% of the time, Pallas kernels for 0%

profile of v1, /device:TPU:0, one launch (start us, length us, event | category | flops | bytes accessed | tf_op | source)
XLA Modules:
  0.0 251.4 jit_solution(14353363218824865677)
XLA Ops:
  7.2 1.1 copy.141
  8.3 14.4 %all_to_all.37 = bf16[16,8,512]{2,0,1:T(8,128)(2,1)S(1)} all-to-all(bf16[16,8,512]{2,0,1:T(8,128)(2,1)S(1)} %bitcast.126), channel_id=1, replica_groups=mesh['ep'=8,'tp'=4] {'ep'}, dimensions={1} | all-to-all | bytes 262144 | tf_op jit(solution)/shard_map/all_to_all | solution.py:97
  22.7 0.8 convolution_bitcast_fusion.1
  23.5 0.7 copy.108
  24.4 2.3 convolution_bitcast_fusion
  26.6 1.3 copy.106
  28.1 6.1 %reshape.183 = f32[16,4,128,128]{3,2,1,0:T(8,128)} reshape(f32[16,4,16384]{2,1,0:T(4,128)} %param.30) | data formatting | bytes 8388608 | tf_op jit(solution)/shard_map/reshape | solution.py:116
  34.7 0.2 select_reduce_fusion
  34.9 49.9 %reduce-scatter.12.cloned.1.call-done = f32[16,8]{1,0:T(8,128)} async-done(((f32[128,8]{1,0:T(8,128)}), f32[16,8]{1,0:T(8,128)}) %reduce-scatter.12.cloned.1.call-update) | async-done | bytes 528 | tf_op jit(solution)/shard_map/reduce_scatter | solution.py:104
  84.8 0.9 broadcast_multiply_fusion.2
  85.7 66.2 %reduce-scatter.10.cloned.1.call-done = f32[16,2048]{1,0:T(8,128)} async-done(((f32[128,2048]{1,0:T(8,128)}), f32[16,2048]{1,0:T(8,128)}) %reduce-scatter.10.cloned.1.call-update) | async-done | bytes 131088
  151.8 1.2 copy.107
  153.1 0.9 fusion.62
  154.0 1.0 copy.111
  155.0 1.1 copy.112
  156.1 1.1 copy.113
  157.2 0.1 bitcast_multiply_fusion.2
  157.3 5.3 %fusion.64 = f32[16,4,1,128]{3,2,1,0:T(1,128)S(1)} fusion(f32[16,4,128,1]{2,3,1,0:T(1,128)S(1)} %bitcast.127, f32[16,4,128,128]{3,2,1,0:T(8,128)} %reshape.183), kind=kOutput, calls=%fused_computation.111 | convolution fusion | flops 12582912 | bytes 4259840 | tf_op jit(solution)/shard_map/bhd,bhde->bhe/dot_general | solution.py:23
  162.7 0.2 multiply_reduce_fusion.2
  162.9 0.1 broadcast_multiply_fusion.1
  163.2 2.8 %convolution_convert_fusion.1 = bf16[16,4096]{1,0:T(8,128)(2,1)S(1)} fusion(bf16[512,4096]{1,0:T(8,128)(2,1)} %param.33, f32[2,8,4,128]{3,2,1,0:T(4,128)S(1)} %bitcast.130, f32[2,8,4,128]{3,2,1,0:T(4,128)S(1)} %bitcast.131, f32[512]{0:T(512)S(1)} %copy-done.6), kind=kOutput, calls=%fused_computation.4 | convolution fusion | flops 67198976 | bytes 4392960 | tf_op jit(solution)/shard_map/dot_general | solution.py:122
  166.0 7.1 %all-gather = bf16[64,4096]{1,0:T(8,128)(2,1)S(1)} all-gather(bf16[16,4096]{1,0:T(8,128)(2,1)S(1)} %convolution_convert_fusion.1), channel_id=2, replica_groups=mesh['ep'=8,'tp'=4] {'tp'}, dimensions={0}, use_global_device_ids=true | all-gather | bytes 655360 | tf_op jit(solution)/shard_map/all_gather | solution.py:126
  173.2 0.2 fusion.27
  173.6 0.2 broadcast_in_dim.15
  173.9 1.8 scatter_custom_fusion
  175.7 3.6 %all-to-all-start.1 = ((bf16[8,8,4096]{2,1,0:T(8,128)(2,1)}), bf16[8,8,4096]{2,1,0:T(8,128)(2,1)S(1)}, u32[]{:S(2)}, u32[]{:S(2)}) async-start(bf16[8,8,4096]{2,1,0:T(8,128)(2,1)} %bitcast.19), calls=%async_computation.1 | async-start | bytes 1048576 | tf_op jit(solution)/shard_map/all_to_all | solution.py:146
  179.2 0.2 reduce-scatter.8.cloned.1.call-start
  179.5 0.7 copy.100
  180.1 2.6 %broadcast_multiply_fusion = f32[16,4,128,128]{3,2,1,0:T(8,128)} fusion(f32[16,4,128]{2,1,0:T(4,128)S(1)} %bitcast.123, f32[16,4,128]{2,1,0:T(4,128)S(1)} %get-tuple-element.25), kind=kLoop, calls=%fused_computation.19 | loop fusion | flops 1048576 | bytes 4259840 | tf_op jit(solution)/shard_map/mul | solution.py:27
  182.7 5.6 %mul.268 = f32[16,4,16384]{2,1,0:T(4,128)} reshape(f32[16,4,128,128]{3,2,1,0:T(8,128)} %broadcast_multiply_fusion) | data formatting | bytes 8388608 | tf_op jit(solution)/shard_map/mul | solution.py:27
  188.3 6.0 %all-to-all-done.1 = bf16[8,8,4096]{2,1,0:T(8,128)(2,1)S(1)} async-done(((bf16[8,8,4096]{2,1,0:T(8,128)(2,1)}), bf16[8,8,4096]{2,1,0:T(8,128)(2,1)S(1)}, u32[]{:S(2)}, u32[]{:S(2)}) %all-to-all-start.1) | async-done | bytes 524320 | tf_op jit(solution)/shard_map/all_to_all | solution.py:146
  194.4 2.0 fusion.11
  196.4 3.8 %fusion = bf16[1,64,4096]{2,1,0:T(8,128)(2,1)} fusion(bf16[1,256,4096]{2,1,0:T(8,128)(2,1)S(1)} %copy-done, bf16[1,4096,256]{2,1,0:T(8,128)(2,1)} %param.39, bf16[8,8,4096]{2,1,0:T(8,128)(2,1)S(1)} %all-to-all-done.1, f32[64,256]{1,0:T(8,128)S(1)} %fusion.11), kind=kOutput, calls=%fused_computation.3 | convolution fusion | flops 268795904 | bytes 5308416 | tf_op jit(solution)/shard_map/erf,efd->erd/dot_general | solution.py:152
  200.3 6.9 %multiply_add_fusion = f32[16,4,16384]{2,1,0:T(4,128)} fusion(f32[16,4,16384]{2,1,0:T(4,128)} %mul.268, f32[16,4,16384]{2,1,0:T(4,128)} %param.30, f32[16,4]{1,0:T(8,128)S(1)} %get-tuple-element.28), kind=kLoop, calls=%fused_computation.5 | loop fusion | flops 2097152 | bytes 12583168 | tf_op jit(solution)/shard_map/add | solution.py:26
  207.1 0.4 fusion.19
  207.5 0.4 select_reduce_fusion.2
  207.9 12.5 %reduce-scatter.8.cloned.1.call-done = bf16[1,64,1024]{2,1,0:T(8,128)(2,1)} async-done(((bf16[1,64,4096]{2,1,0:T(8,128)(2,1)}), bf16[1,64,1024]{2,1,0:T(8,128)(2,1)}) %reduce-scatter.8.cloned.1.call-update) | async-done | bytes 131088 | tf_op jit(solution)/shard_map/reduce_scatter | solution.py:155
  220.4 1.1 copy.143
  221.5 0.5 broadcast.198
  222.0 1.4 reduce.1
  223.4 0.7 reshape.218
  224.2 5.5 %all-to-all-start.2 = ((bf16[8,2,4096]{2,1,0:T(2,128)(2,1)}), bf16[8,2,4096]{2,1,0:T(2,128)(2,1)S(1)}, u32[]{:S(2)}, u32[]{:S(2)}) async-start(bf16[8,2,4096]{2,1,0:T(2,128)(2,1)} %reshape.218), calls=%async_computation.3 | async-start | bytes 262144 | tf_op jit(solution)/shard_map/all_to_all | solution.py:158
  229.7 7.3 %all-to-all-done.2 = bf16[8,2,4096]{2,1,0:T(2,128)(2,1)S(1)} async-done(((bf16[8,2,4096]{2,1,0:T(2,128)(2,1)}), bf16[8,2,4096]{2,1,0:T(2,128)(2,1)S(1)}, u32[]{:S(2)}, u32[]{:S(2)}) %all-to-all-start.2) | async-done | bytes 131104 | tf_op jit(solution)/shard_map/all_to_all | solution.py:158
  237.0 0.1 reshape.219
  237.2 0.6 gather_fusion
  238.0 0.2 fusion.59
  238.2 5.9 %all-reduce = (f32[16]{0:T(128)S(1)}, f32[16]{0:T(128)S(1)}) all-reduce(f32[16]{0:T(128)S(1)} %get-tuple-element.9, f32[16]{0:T(128)S(1)} %get-tuple-element.8), channel_id=1, replica_groups=mesh['ep'=8,'tp'=4] {'tp'}, use_global_device_ids=true, to_apply=%region_17.18 | all-reduce | flops 32 | bytes 256 | tf_op jit(solution)/shard_map/psum | solution.py:163
  244.2 0.7 multiply_convert_fusion
  (55 shorter events, 1.6 us)
Async XLA Ops:
  7.2 189.3 %copy-start = (bf16[1,256,4096]{2,1,0:T(8,128)(2,1)S(1)}, bf16[1,256,4096]{2,1,0:T(8,128)(2,1)}, u32[]{:S(2)}) copy-start(bf16[1,256,4096]{2,1,0:T(8,128)(2,1)} %param.40) | copy-start | bytes 6291460
  7.2 77.6 %reduce-scatter.12.cloned.1.call-start = ((), (), s32[]{:S(2)}) async-start(), calls=%async_computation.8 | async-start | bytes 73728 | tf_op jit(solution)/shard_map/reduce_scatter | solution.py:104
  24.3 3.7 %copy-start.9 = (f32[16,4]{0,1:T(4,128)S(1)}, f32[16,4]{0,1:T(4,128)}, u32[]{:S(2)}) copy-start(f32[16,4]{0,1:T(4,128)} %param.31) | copy-start | bytes 772
  24.3 127.5 %reduce-scatter.10.cloned.1.call-start = ((), (), s32[]{:S(2)}) async-start(), calls=%async_computation.7 | async-start | bytes 1179648
  28.1 6.1 %copy-start.4 = (s32[16,2]{0,1:T(2,128)S(1)}, s32[16,2]{0,1:T(2,128)}, u32[]{:S(2)}) copy-start(s32[16,2]{0,1:T(2,128)} %param.37) | copy-start | bytes 388
  28.1 56.7 %copy-start.7 = (f32[4]{0:T(128)S(1)}, f32[4]{0:T(128)}, u32[]{:S(2)}) copy-start(f32[4]{0:T(128)} %param.28) | copy-start | bytes 52
  28.1 56.7 %copy-start.8 = (f32[4]{0:T(128)S(1)}, f32[4]{0:T(128)}, u32[]{:S(2)}) copy-start(f32[4]{0:T(128)} %param.29) | copy-start | bytes 52
  85.7 76.9 %copy-start.2 = (f32[16,8]{1,0:T(8,128)S(1)}, f32[16,8]{1,0:T(8,128)}, u32[]{:S(2)}) copy-start(f32[16,8]{1,0:T(8,128)} %reduce-scatter.12.cloned.1.call-done) | copy-start | bytes 1540
  153.1 10.1 %copy-start.6 = (f32[512]{0:T(512)S(1)}, f32[512]{0:T(512)}, u32[]{:S(2)}) copy-start(f32[512]{0:T(512)} %param.32) | copy-start | bytes 6148
  162.6 10.7 %copy-start.1 = (bf16[16,4096]{1,0:T(8,128)(2,1)S(1)}, bf16[16,4096]{1,0:T(8,128)(2,1)}, u32[]{:S(2)}) copy-start(bf16[16,4096]{1,0:T(8,128)(2,1)} %param.21) | copy-start | bytes 393220
  162.6 10.9 %copy-start.3 = (f32[4096]{0:T(1024)S(1)}, f32[4096]{0:T(1024)}, u32[]{:S(2)}) copy-start(f32[4096]{0:T(1024)} %param.34) | copy-start | bytes 49156
  175.7 18.7 %all-to-all-start.1 = ((bf16[8,8,4096]{2,1,0:T(8,128)(2,1)}), bf16[8,8,4096]{2,1,0:T(8,128)(2,1)S(1)}, u32[]{:S(2)}, u32[]{:S(2)}) async-start(bf16[8,8,4096]{2,1,0:T(8,128)(2,1)} %bitcast.19), calls=%async_computation.1 | async-start | bytes 1048576 | tf_op jit(solution)/shard_map/all_to_all | solution.py:146
  179.2 41.2 %reduce-scatter.8.cloned.1.call-start = ((), (), s32[]{:S(2)}) async-start(), calls=%async_computation.6 | async-start | bytes 655360 | tf_op jit(solution)/shard_map/reduce_scatter | solution.py:155
  200.2 6.9 %copy-start.11 = (bf16[4096,2]{0,1:T(2,128)(2,1)S(1)}, bf16[4096,2]{0,1:T(2,128)(2,1)}, u32[]{:S(2)}) copy-start(bf16[4096,2]{0,1:T(2,128)(2,1)} %param.35) | copy-start | bytes 49156
  200.2 7.3 %copy-start.10 = (bf16[4096,8]{0,1:T(8,128)(2,1)S(1)}, bf16[4096,8]{0,1:T(8,128)(2,1)}, u32[]{:S(2)}) copy-start(bf16[4096,8]{0,1:T(8,128)(2,1)} %param.36) | copy-start | bytes 196612
  207.1 37.1 %copy-start.5 = (f32[1024]{0:T(1024)S(1)}, f32[1024]{0:T(1024)}, u32[]{:S(2)}) copy-start(f32[1024]{0:T(1024)} %param.41) | copy-start | bytes 12292
  224.2 12.9 %all-to-all-start.2 = ((bf16[8,2,4096]{2,1,0:T(2,128)(2,1)}), bf16[8,2,4096]{2,1,0:T(2,128)(2,1)S(1)}, u32[]{:S(2)}, u32[]{:S(2)}) async-start(bf16[8,2,4096]{2,1,0:T(2,128)(2,1)} %reshape.218), calls=%async_computation.3 | async-start | bytes 262144 | tf_op jit(solution)/shard_map/all_to_all | solution.py:158
Sparse Core Ops, SparseCore 0:
  24.4 60.3 reduce-scatter.11
  88.2 63.5 reduce-scatter.9
  200.4 20.0 reduce-scatter.7
